TPU v7x, 512 devices: a 8x2x16 block of a 8x16x16 slice. The times are simulated.
512 devices in a mesh: grp: 2 (over y), fs: 16 (over z), tp: 16 (over x, core).
Axes of the slice: x: 8, y: 2, z: 16, core: 2. Of those that a mesh axis runs over, the one named last changes fastest.
The devices are a block of a 8x16x16 slice.
Arguments:
- tokens: bfloat16 [4096, 2048], P(('grp', 'fs')), parts along dimension 0, may hold values from -12 to 12, as said below
- mix_heads: bfloat16 [4096, 2048], P(('grp', 'fs'), 'tp'), parts along dimension 0, may hold values from -6 to 6
- norm_first: float32 [2048], replicated, may hold values from 0.1 to 1.9
- gate_first: bfloat16 [2048, 5632], P('fs', 'tp'), may hold values from -0.125 to 0.125
- up_first: bfloat16 [2048, 5632], P('fs', 'tp'), may hold values from -0.125 to 0.125
- down_first: bfloat16 [5632, 2048], P('tp', 'fs'), may hold values from -0.078125 to 0.078125
- out_weight: bfloat16 [2048, 2048], P('tp', 'fs'), may hold values from -0.125 to 0.125
- norm_second: float32 [2048], replicated, may hold values from 0.1 to 1.9
- gate_second: bfloat16 [2048, 5632], P('fs', 'tp'), may hold values from -0.125 to 0.125
- up_second: bfloat16 [2048, 5632], P('fs', 'tp'), may hold values from -0.125 to 0.125
- down_second: bfloat16 [5632, 2048], P('tp', 'fs'), may hold values from -0.078125 to 0.078125
Outputs:
- layer_out: bfloat16 [4096, 2048], P(('grp', 'fs')), parts along dimension 0
There are 2 independent parts, one for each index of `grp`. A program takes and returns all parts, laid end to end along the dimension named above; an argument that names none is the same for every part. Nothing has to cross between parts.
Inputs may be any that keep to these rules, and one draw needn't show every extreme that they name: Each row of tokens carries a scale of its own.
All inputs are finite; a program needn't handle non-finite values.
Results may differ from a plain program's by a relative error of at most 0.014.
Values may be sent and summed in bfloat16 or wider, within the bound.
A program may use at most 64 MiB of HBM per device.

v0:
```python
import jax
import jax.numpy as jnp
from jax import lax
from jax.sharding import PartitionSpec as P

EPS = 0.1


def side_by_side(arrays, axis, dim, along):
    both = jnp.concatenate(arrays, axis=along)
    result, at, done = (lax.all_gather(both, axis, axis=dim, tiled=True), 0, [])
    for a in arrays:
        done.append(lax.slice_in_dim(result, at, at + a.shape[along], axis=along))
        at += a.shape[along]
    return tuple(done)


def laid_out(tiles, dim):
    lengths = list(tiles.shape[1:])
    lengths[dim] *= tiles.shape[0]
    return jnp.moveaxis(tiles, 0, dim).reshape(lengths)


def sent_to_all(array, axis):
    size = lax.axis_size(axis)
    return lax.all_to_all(
        jnp.broadcast_to(array[None], (size, *array.shape)), axis, 0, 0, tiled=True
    )


def gather_directly(array, axis, dim):
    return laid_out(sent_to_all(array, axis), dim)


def in_blocks(array, dim, size):
    before, after = (array.shape[:dim], array.shape[dim + 1 :])
    return jnp.moveaxis(array.reshape(*before, size, -1, *after), dim, 0)


def sum_at_owner(array, axis, dim):
    size = lax.axis_size(axis)
    tiles = lax.all_to_all(in_blocks(array, dim, size), axis, 0, 0, tiled=True)
    return jnp.sum(tiles.astype(jnp.float32), axis=0)


def norm_rows(row_block, gain_vector):
    widened = row_block.astype(jnp.float32)
    scaled = widened * lax.rsqrt(jnp.mean(widened * widened, axis=-1, keepdims=True) + EPS)
    return (scaled * gain_vector).astype(jnp.bfloat16)


def gate_values(normed, gate_weight, value_weight):
    pieces = side_by_side((gate_weight, value_weight), "fs", 0, 1)
    return (
        jnp.dot(normed, pieces[0], preferred_element_type=jnp.float32),
        jnp.dot(normed, pieces[1], preferred_element_type=jnp.float32),
    )


def half_branch(normed, gate_weight, value_weight, down_weight):
    gates, values = gate_values(normed, gate_weight, value_weight)
    hidden = (jax.nn.silu(gates) * values).astype(jnp.bfloat16)
    return 0.5 * jnp.dot(
        hidden, gather_directly(down_weight, "fs", 1), preferred_element_type=jnp.float32
    )


def share_sum(block_terms):
    return sum_at_owner(block_terms.astype(jnp.bfloat16), "tp", 0)


def join_rows(row_block):
    return lax.all_gather(row_block, "tp", axis=0, tiled=True)


def local(
    tokens,
    mix_heads,
    norm_first,
    gate_first,
    up_first,
    down_first,
    out_weight,
    norm_second,
    gate_second,
    up_second,
    down_second,
):
    normed_one = norm_rows(tokens, norm_first)
    first_terms = half_branch(normed_one, gate_first, up_first, down_first)
    heads_out = jnp.dot(
        mix_heads, gather_directly(out_weight, "fs", 1), preferred_element_type=jnp.float32
    )
    first_terms = first_terms + heads_out
    share_rows = tokens.shape[0] // lax.axis_size("tp")
    offset = lax.axis_index("tp") * share_rows
    own_rows = lax.dynamic_slice_in_dim(tokens, offset, share_rows, 0).astype(jnp.float32)
    resid_two = own_rows + share_sum(first_terms)
    normed_two = join_rows(norm_rows(resid_two, norm_second))
    second_terms = half_branch(normed_two, gate_second, up_second, down_second)
    finished = (resid_two + share_sum(second_terms)).astype(jnp.bfloat16)
    return join_rows(finished)


def solution(mesh):
    in_specs = (
        P(("grp", "fs"), None),
        P(("grp", "fs"), "tp"),
        P(),
        P("fs", "tp"),
        P("fs", "tp"),
        P("tp", "fs"),
        P("tp", "fs"),
        P(),
        P("fs", "tp"),
        P("fs", "tp"),
        P("tp", "fs"),
    )
    out_specs = P(("grp", "fs"), None)
    return jax.shard_map(local, mesh=mesh, in_specs=in_specs, out_specs=out_specs, check_vma=False)
```

profile of v0, /device:TPU:65, one launch (start us, length us, event | category | flops | bytes accessed | tf_op | source)
XLA Modules:
  0.0 398.9 jit_solution(9208464378308235055)
XLA Ops:
  6.6 2.2 broadcast_in_dim.6
  8.8 44.4 %all-to-all-start = ((bf16[16,352,128]{2,1,0:T(8,128)(2,1)}), bf16[16,352,128]{2,1,0:T(8,128)(2,1)S(1)}, u32[]{:S(2)}, u32[]{:S(2)}) async-start(bf16[16,352,128]{2,1,0:T(8,128)(2,1)} %broadcast_in_dim.6), calls=%async_computation | async-start | bytes 2883584 | tf_op jit(solution)/shard_map/all_to_all | solution.py:26
  54.1 68.0 %all-to-all-done = bf16[16,352,128]{2,1,0:T(8,128)(2,1)S(1)} async-done(((bf16[16,352,128]{2,1,0:T(8,128)(2,1)}), bf16[16,352,128]{2,1,0:T(8,128)(2,1)S(1)}, u32[]{:S(2)}, u32[]{:S(2)}) %all-to-all-start) | async-done | bytes 1441824 | tf_op jit(solution)/shard_map/all_to_all | solution.py:26
  122.1 0.9 broadcast_in_dim.7
  123.0 13.5 %all-to-all-start.1 = ((bf16[16,128,128]{1,2,0:T(8,128)(2,1)}), bf16[16,128,128]{1,2,0:T(8,128)(2,1)S(1)}, u32[]{:S(2)}, u32[]{:S(2)}) async-start(bf16[16,128,128]{1,2,0:T(8,128)(2,1)} %broadcast_in_dim.7), calls=%async_computation.1 | async-start | bytes 1048576 | tf_op jit(solution)/shard_map/all_to_all | solution.py:26
  136.8 48.7 %all-gather.3.cloned.1.call-done = bf16[2048,704]{0,1:T(8,128)(2,1)} async-done(((bf16[128,704]{0,1:T(8,128)(2,1)}), bf16[2048,704]{0,1:T(8,128)(2,1)}) %all-gather.3.cloned.1.call-update) | async-done | bytes 2883600 | tf_op jit(solution)/shard_map/all_gather | solution.py:11
  185.5 2.0 fusion.14
  187.5 3.1 convolution_multiply_fusion.1
  190.6 1.1 fusion.3
  191.7 15.7 %all-to-all-start.2 = ((bf16[16,8,2048]{2,1,0:T(8,128)(2,1)}), bf16[16,8,2048]{2,1,0:T(8,128)(2,1)S(1)}, u32[]{:S(2)}, u32[]{:S(2)}) async-start(bf16[16,8,2048]{2,1,0:T(8,128)(2,1)} %fusion.3), calls=%async_computation.2 | async-start | bytes 1048576 | tf_op jit(solution)/shard_map/all_to_all | solution.py:42
  207.5 0.7 pad_maximum_fusion.1
  208.3 16.4 %all-to-all-done.2 = bf16[16,8,2048]{2,1,0:T(8,128)(2,1)S(1)} async-done(((bf16[16,8,2048]{2,1,0:T(8,128)(2,1)}), bf16[16,8,2048]{2,1,0:T(8,128)(2,1)S(1)}, u32[]{:S(2)}, u32[]{:S(2)}) %all-to-all-start.2) | async-done | bytes 524320 | tf_op jit(solution)/shard_map/all_to_all | solution.py:42
  224.6 1.3 broadcast_in_dim.8
  225.9 8.3 %all-to-all-start.3 = ((bf16[16,352,128]{2,1,0:T(8,128)(2,1)}), bf16[16,352,128]{2,1,0:T(8,128)(2,1)S(1)}, u32[]{:S(2)}, u32[]{:S(2)}) async-start(bf16[16,352,128]{2,1,0:T(8,128)(2,1)} %broadcast_in_dim.8), calls=%async_computation.3 | async-start | bytes 2883584 | tf_op jit(solution)/shard_map/all_to_all | solution.py:26
  234.3 0.9 multiply_reduce_fusion
  235.2 0.8 multiply_convert_fusion
  236.0 16.0 %all_gather.13 = bf16[128,2048]{1,0:T(8,128)(2,1)S(1)} all-gather(bf16[8,2048]{1,0:T(8,128)(2,1)S(1)} %multiply_convert_fusion), channel_id=1, replica_groups=mesh['grp'=2,'fs'=16,'tp'=16] {'tp'}, dimensions={0}, use_global_device_ids=true | all-gather | bytes 557056 | tf_op jit(solution)/shard_map/all_gather | solution.py:73
  252.0 86.3 %all-gather.5.cloned.1.call-done = bf16[2048,704]{0,1:T(8,128)(2,1)} async-done(((bf16[128,704]{0,1:T(8,128)(2,1)}), bf16[2048,704]{0,1:T(8,128)(2,1)}) %all-gather.5.cloned.1.call-update) | async-done | bytes 2883600 | tf_op jit(solution)/shard_map/all_gather | solution.py:11
  338.3 1.9 fusion.10
  340.2 2.8 fusion.2
  343.1 31.3 %all_to_all.25 = bf16[16,8,2048]{2,1,0:T(8,128)(2,1)S(1)} all-to-all(bf16[16,8,2048]{2,1,0:T(8,128)(2,1)S(1)} %fusion.2), channel_id=1, replica_groups=mesh['grp'=2,'fs'=16,'tp'=16] {'tp'}, dimensions={0} | all-to-all | bytes 1048576 | tf_op jit(solution)/shard_map/all_to_all | solution.py:42
  374.5 0.8 add_convert_fusion
  375.2 16.0 %all_gather.15 = bf16[128,2048]{1,0:T(8,128)(2,1)S(1)} all-gather(bf16[8,2048]{1,0:T(8,128)(2,1)S(1)} %add_convert_fusion), channel_id=1, replica_groups=mesh['grp'=2,'fs'=16,'tp'=16] {'tp'}, dimensions={0}, use_global_device_ids=true | all-gather | bytes 557056 | tf_op jit(solution)/shard_map/all_gather | solution.py:73
  391.2 0.8 copy.27
  (33 shorter events, 1.4 us)
Async XLA Ops:
  6.5 184.0 %copy-start = (bf16[128,128]{1,0:T(8,128)(2,1)S(1)}, bf16[128,128]{1,0:T(8,128)(2,1)}, u32[]{:S(2)}) copy-start(bf16[128,128]{1,0:T(8,128)(2,1)} %param.12) | copy-start | bytes 98308
  8.8 44.5 %copy-start.2 = (bf16[128,352]{0,1:T(8,128)(2,1)S(1)}, bf16[128,352]{0,1:T(8,128)(2,1)}, u32[]{:S(2)}) copy-start(bf16[128,352]{0,1:T(8,128)(2,1)} %param.15) | copy-start | bytes 270340
  8.8 44.5 %copy-start.3 = (bf16[128,352]{0,1:T(8,128)(2,1)S(1)}, bf16[128,352]{0,1:T(8,128)(2,1)}, u32[]{:S(2)}) copy-start(bf16[128,352]{0,1:T(8,128)(2,1)} %param.14) | copy-start | bytes 270340
  8.8 45.2 %copy-start.7 = (bf16[128,128]{1,0:T(8,128)(2,1)S(1)}, bf16[128,128]{1,0:T(8,128)(2,1)}, u32[]{:S(2)}) copy-start(bf16[128,128]{1,0:T(8,128)(2,1)} %param.17) | copy-start | bytes 98308
  8.8 113.4 %all-to-all-start = ((bf16[16,352,128]{2,1,0:T(8,128)(2,1)}), bf16[16,352,128]{2,1,0:T(8,128)(2,1)S(1)}, u32[]{:S(2)}, u32[]{:S(2)}) async-start(bf16[16,352,128]{2,1,0:T(8,128)(2,1)} %broadcast_in_dim.6), calls=%async_computation | async-start | bytes 2883584 | tf_op jit(solution)/shard_map/all_to_all | solution.py:26
  53.1 83.4 %copy-start.1 = (bf16[128,2048]{1,0:T(8,128)(2,1)S(1)}, bf16[128,2048]{1,0:T(8,128)(2,1)}, u32[]{:S(2)}) copy-start(bf16[128,2048]{1,0:T(8,128)(2,1)} %param.11) | copy-start | bytes 1572868
  53.1 132.4 %copy-start.9 = (f32[2048]{0:T(1024)S(1)}, f32[2048]{0:T(1024)}, u32[]{:S(2)}) copy-start(f32[2048]{0:T(1024)} %param.13) | copy-start | bytes 24580
  53.1 132.3 %all-gather.3.cloned.1.call-start = ((), (), s32[]{:S(2)}) async-start(), calls=%async_computation.5 | async-start | bytes 3063808 | tf_op jit(solution)/shard_map/all_gather | solution.py:11
  123.0 67.6 %all-to-all-start.1 = ((bf16[16,128,128]{1,2,0:T(8,128)(2,1)}), bf16[16,128,128]{1,2,0:T(8,128)(2,1)S(1)}, u32[]{:S(2)}, u32[]{:S(2)}) async-start(bf16[16,128,128]{1,2,0:T(8,128)(2,1)} %broadcast_in_dim.7), calls=%async_computation.1 | async-start | bytes 1048576 | tf_op jit(solution)/shard_map/all_to_all | solution.py:26
  190.6 16.9 %copy-start.4 = (bf16[128,352]{0,1:T(8,128)(2,1)S(1)}, bf16[128,352]{0,1:T(8,128)(2,1)}, u32[]{:S(2)}) copy-start(bf16[128,352]{0,1:T(8,128)(2,1)} %param.20) | copy-start | bytes 270340
  190.6 16.9 %copy-start.5 = (bf16[128,352]{0,1:T(8,128)(2,1)S(1)}, bf16[128,352]{0,1:T(8,128)(2,1)}, u32[]{:S(2)}) copy-start(bf16[128,352]{0,1:T(8,128)(2,1)} %param.19) | copy-start | bytes 270340
  190.6 34.0 %copy-start.6 = (bf16[352,128]{1,0:T(8,128)(2,1)S(1)}, bf16[352,128]{1,0:T(8,128)(2,1)}, u32[]{:S(2)}) copy-start(bf16[352,128]{1,0:T(8,128)(2,1)} %param.21) | copy-start | bytes 270340
  191.7 32.9 %all-to-all-start.2 = ((bf16[16,8,2048]{2,1,0:T(8,128)(2,1)}), bf16[16,8,2048]{2,1,0:T(8,128)(2,1)S(1)}, u32[]{:S(2)}, u32[]{:S(2)}) async-start(bf16[16,8,2048]{2,1,0:T(8,128)(2,1)} %fusion.3), calls=%async_computation.2 | async-start | bytes 1048576 | tf_op jit(solution)/shard_map/all_to_all | solution.py:42
  207.4 130.9 %all-gather.5.cloned.1.call-start = ((), (), s32[]{:S(2)}) async-start(), calls=%async_computation.6 | async-start | bytes 3063808 | tf_op jit(solution)/shard_map/all_gather | solution.py:11
  225.9 9.3 %copy-start.8 = (f32[2048]{0:T(1024)S(1)}, f32[2048]{0:T(1024)}, u32[]{:S(2)}) copy-start(f32[2048]{0:T(1024)} %param.18) | copy-start | bytes 24580
  225.9 114.3 %all-to-all-start.3 = ((bf16[16,352,128]{2,1,0:T(8,128)(2,1)}), bf16[16,352,128]{2,1,0:T(8,128)(2,1)S(1)}, u32[]{:S(2)}, u32[]{:S(2)}) async-start(bf16[16,352,128]{2,1,0:T(8,128)(2,1)} %broadcast_in_dim.8), calls=%async_computation.3 | async-start | bytes 2883584 | tf_op jit(solution)/shard_map/all_to_all | solution.py:26
Sparse Core Ops, SparseCore 0:
  56.0 129.4 all-gather.2
  210.3 127.9 all-gather.4
where the time goes:
time: 400 us; the launch traced here: 399 us
  waiting for transfers between devices  220 us (55%)
  starting transfers between devices  82 us (20%)
  blocking collectives  63.3 us (16%)
  between operations  13.6 us (3%)
  matrix products  10.9 us (3%)
  local copies, waits for them, and re-layouts  5.35 us (1%)
  other arithmetic  4.25 us (1%)
    all_gather x2, waiting for transfers between devices, side_by_side(): result, at, done = (lax.all_gather(both, axis, axis=dim, tiled=True), 0, [])  135 us
    all_to_all x3, waiting for transfers between devices, sent_to_all(): lax.all_to_all(jnp.broadcast_to(array[None], (size, *array.shape)), axis,...  68 us
    all_to_all x3, starting transfers between devices, sent_to_all(): lax.all_to_all(jnp.broadcast_to(array[None], (size, *array.shape)), axis,...  66.1 us
    all_gather x2, blocking collectives, join_rows(): return lax.all_gather(row_block, 'tp', axis=0, tiled=True)  32 us
    all_to_all x1, blocking collectives, sum_at_owner(): tiles = lax.all_to_all(in_blocks(array, dim, size), axis, 0, 0, tiled=True)  31.3 us
    all_to_all x1, waiting for transfers between devices, sum_at_owner(): tiles = lax.all_to_all(in_blocks(array, dim, size), axis, 0, 0, tiled=True)  16.4 us
    all_to_all x1, starting transfers between devices, sum_at_owner(): tiles = lax.all_to_all(in_blocks(array, dim, size), axis, 0, 0, tiled=True)  15.7 us
  transfers between devices with their start and end apart: 6, of which 4 were waited for; matrix products, arithmetic and copies ran while one was open for 3% of the time, Pallas kernels for 0%

commit v1 on v0

--- a/solution.py
+++ b/solution.py
@@ -4,6 +4,19 @@
 from jax.sharding import PartitionSpec as P
 
 EPS = 0.1
+
+
+def collect(array, axis, dim):
+    ways = lax.axis_size(axis)
+    up = [(d, (d + 1) % ways) for d in range(ways)]
+    down = [(d, (d - 1) % ways) for d in range(ways)]
+    earlier, later = ([array], [array])
+    for _ in range(ways // 2):
+        earlier.append(lax.ppermute(earlier[-1], axis, up))
+    for _ in range((ways - 1) // 2):
+        later.append(lax.ppermute(later[-1], axis, down))
+    line = jnp.concatenate([*earlier[::-1], *later[1:]], axis=dim)
+    return jnp.roll(line, (lax.axis_index(axis) - ways // 2) * array.shape[dim], axis=dim)
 
 
 def side_by_side(arrays, axis, dim, along):
@@ -70,7 +83,7 @@
 
 
 def join_rows(row_block):
-    return lax.all_gather(row_block, "tp", axis=0, tiled=True)
+    return collect(row_block, "tp", 0)
 
 
 def local(

time: 400 us -> 418 us (1.045)
  starting transfers between devices: 82 us -> 131 us
  blocking collectives: 63.3 us -> 31.1 us
    ppermute x0 -> x30, starting transfers between devices: none -> 48.9 us  [the longest x14 37.1 us: collect(): later.append(lax.ppermute(later[-1], axis, down))]
    all_gather x2 -> x0, blocking collectives: 32 us -> none  [join_rows(): return lax.all_gather(row_block, 'tp', axis=0, tiled=True)]
    all_gather x2, waiting for transfers between devices: 135 us -> 117 us  [side_by_side(): result, at, done = (lax.all_gather(both, axis, axis=dim, tiled=True), 0, [])]
    ppermute x0 -> x30, waiting for transfers between devices: none -> 16.2 us  [the longest x16 9.23 us: collect(): earlier.append(lax.ppermute(earlier[-1], axis, up))]
  transfers between devices with their start and end apart: 6 -> 36, of which waited for: 4 -> 29; matrix products, arithmetic and copies ran while one was open for 3% -> 3% of each run, Pallas kernels for 0% -> 0%
where the time goes in v1:
time: 418 us; the launch traced here: 415 us
  waiting for transfers between devices  218 us (52%)
  starting transfers between devices  131 us (31%)
  blocking collectives  31.1 us (7%)
  between operations  13.9 us (3%)
  matrix products  11.1 us (3%)
  other arithmetic  5.35 us (1%)
  local copies, waits for them, and re-layouts  4.69 us (1%)
    all_gather x2, waiting for transfers between devices, side_by_side(): result, at, done = (lax.all_gather(both, axis, axis=dim, tiled=True), 0, [])  117 us
    all_to_all x3, waiting for transfers between devices, sent_to_all(): lax.all_to_all(jnp.broadcast_to(array[None], (size, *array.shape)), axis,...  68 us
    all_to_all x3, starting transfers between devices, sent_to_all(): lax.all_to_all(jnp.broadcast_to(array[None], (size, *array.shape)), axis,...  66.1 us
    ppermute x14, starting transfers between devices, collect(): later.append(lax.ppermute(later[-1], axis, down))  37.1 us
    all_to_all x1, blocking collectives, sum_at_owner(): tiles = lax.all_to_all(in_blocks(array, dim, size), axis, 0, 0, tiled=True)  31.1 us
    all_to_all x1, waiting for transfers between devices, sum_at_owner(): tiles = lax.all_to_all(in_blocks(array, dim, size), axis, 0, 0, tiled=True)  16.4 us
    all_to_all x1, starting transfers between devices, sum_at_owner(): tiles = lax.all_to_all(in_blocks(array, dim, size), axis, 0, 0, tiled=True)  15.7 us
    ppermute x16, starting transfers between devices, collect(): earlier.append(lax.ppermute(earlier[-1], axis, up))  11.8 us
  transfers between devices with their start and end apart: 36, of which 29 were waited for; matrix products, arithmetic and copies ran while one was open for 3% of the time, Pallas kernels for 0%

profile of v1, /device:TPU:65, one launch (start us, length us, event | category | flops | bytes accessed | tf_op | source)
XLA Modules:
  0.0 414.9 jit_solution(5712282073954802865)
XLA Ops:
  6.6 2.2 broadcast_in_dim.6
  8.8 44.4 %all-to-all-start = ((bf16[16,352,128]{2,1,0:T(8,128)(2,1)}), bf16[16,352,128]{2,1,0:T(8,128)(2,1)S(1)}, u32[]{:S(2)}, u32[]{:S(2)}) async-start(bf16[16,352,128]{2,1,0:T(8,128)(2,1)} %broadcast_in_dim.6), calls=%async_computation | async-start | bytes 2883584 | tf_op jit(solution)/shard_map/all_to_all | solution.py:39
  54.1 68.0 %all-to-all-done = bf16[16,352,128]{2,1,0:T(8,128)(2,1)S(1)} async-done(((bf16[16,352,128]{2,1,0:T(8,128)(2,1)}), bf16[16,352,128]{2,1,0:T(8,128)(2,1)S(1)}, u32[]{:S(2)}, u32[]{:S(2)}) %all-to-all-start) | async-done | bytes 1441824 | tf_op jit(solution)/shard_map/all_to_all | solution.py:39
  123.0 13.5 %all-to-all-start.1 = ((bf16[16,128,128]{1,2,0:T(8,128)(2,1)}), bf16[16,128,128]{1,2,0:T(8,128)(2,1)S(1)}, u32[]{:S(2)}, u32[]{:S(2)}) async-start(bf16[16,128,128]{1,2,0:T(8,128)(2,1)} %broadcast_in_dim.7), calls=%async_computation.1 | async-start | bytes 1048576 | tf_op jit(solution)/shard_map/all_to_all | solution.py:39
  136.8 48.7 %all-gather.3.cloned.1.call-done = bf16[2048,704]{0,1:T(8,128)(2,1)} async-done(((bf16[128,704]{0,1:T(8,128)(2,1)}), bf16[2048,704]{0,1:T(8,128)(2,1)}) %all-gather.3.cloned.1.call-update) | async-done | bytes 2883600 | tf_op jit(solution)/shard_map/all_gather | solution.py:24
  187.5 3.1 convolution_multiply_fusion.1
  191.7 15.7 %all-to-all-start.2 = ((bf16[16,8,2048]{2,1,0:T(8,128)(2,1)}), bf16[16,8,2048]{2,1,0:T(8,128)(2,1)S(1)}, u32[]{:S(2)}, u32[]{:S(2)}) async-start(bf16[16,8,2048]{2,1,0:T(8,128)(2,1)} %fusion.3), calls=%async_computation.2 | async-start | bytes 1048576 | tf_op jit(solution)/shard_map/all_to_all | solution.py:55
  208.2 16.4 %all-to-all-done.2 = bf16[16,8,2048]{2,1,0:T(8,128)(2,1)S(1)} async-done(((bf16[16,8,2048]{2,1,0:T(8,128)(2,1)}), bf16[16,8,2048]{2,1,0:T(8,128)(2,1)S(1)}, u32[]{:S(2)}, u32[]{:S(2)}) %all-to-all-start.2) | async-done | bytes 524320 | tf_op jit(solution)/shard_map/all_to_all | solution.py:55
  225.9 8.3 %all-to-all-start.3 = ((bf16[16,352,128]{2,1,0:T(8,128)(2,1)}), bf16[16,352,128]{2,1,0:T(8,128)(2,1)S(1)}, u32[]{:S(2)}, u32[]{:S(2)}) async-start(bf16[16,352,128]{2,1,0:T(8,128)(2,1)} %broadcast_in_dim.8), calls=%async_computation.3 | async-start | bytes 2883584 | tf_op jit(solution)/shard_map/all_to_all | solution.py:39
  240.4 2.3 collective-permute-start.2
  246.9 2.3 collective-permute-start.10
  250.6 3.5 collective-permute-start.11
  255.0 4.1 collective-permute-start.12
  260.0 4.1 collective-permute-start.13
  264.9 4.1 collective-permute-start.14
  269.9 68.6 %all-gather.5.cloned.1.call-done = bf16[2048,704]{0,1:T(8,128)(2,1)} async-done(((bf16[128,704]{0,1:T(8,128)(2,1)}), bf16[2048,704]{0,1:T(8,128)(2,1)}) %all-gather.5.cloned.1.call-update) | async-done | bytes 2883600 | tf_op jit(solution)/shard_map/all_gather | solution.py:24
  340.5 2.9 fusion.2
  343.4 31.1 %all_to_all.25 = bf16[16,8,2048]{2,1,0:T(8,128)(2,1)S(1)} all-to-all(bf16[16,8,2048]{2,1,0:T(8,128)(2,1)S(1)} %fusion.2), channel_id=1, replica_groups=mesh['grp'=2,'fs'=16,'tp'=16] {'tp'}, dimensions={0} | all-to-all | bytes 1048576 | tf_op jit(solution)/shard_map/all_to_all | solution.py:55
  379.8 2.3 collective-permute-start.17
  385.7 2.2 collective-permute-start.25
  389.1 3.4 collective-permute-start.26
  393.3 3.7 collective-permute-start.27
  397.9 3.7 collective-permute-start.28
  402.4 3.7 collective-permute-start.29
  (123 shorter events, 38.9 us)
Async XLA Ops:
  8.8 113.4 %all-to-all-start = ((bf16[16,352,128]{2,1,0:T(8,128)(2,1)}), bf16[16,352,128]{2,1,0:T(8,128)(2,1)S(1)}, u32[]{:S(2)}, u32[]{:S(2)}) async-start(bf16[16,352,128]{2,1,0:T(8,128)(2,1)} %broadcast_in_dim.6), calls=%async_computation | async-start | bytes 2883584 | tf_op jit(solution)/shard_map/all_to_all | solution.py:39
  53.1 132.3 %all-gather.3.cloned.1.call-start = ((), (), s32[]{:S(2)}) async-start(), calls=%async_computation.5 | async-start | bytes 3063808 | tf_op jit(solution)/shard_map/all_gather | solution.py:24
  123.0 67.6 %all-to-all-start.1 = ((bf16[16,128,128]{1,2,0:T(8,128)(2,1)}), bf16[16,128,128]{1,2,0:T(8,128)(2,1)S(1)}, u32[]{:S(2)}, u32[]{:S(2)}) async-start(bf16[16,128,128]{1,2,0:T(8,128)(2,1)} %broadcast_in_dim.7), calls=%async_computation.1 | async-start | bytes 1048576 | tf_op jit(solution)/shard_map/all_to_all | solution.py:39
  191.7 32.9 %all-to-all-start.2 = ((bf16[16,8,2048]{2,1,0:T(8,128)(2,1)}), bf16[16,8,2048]{2,1,0:T(8,128)(2,1)S(1)}, u32[]{:S(2)}, u32[]{:S(2)}) async-start(bf16[16,8,2048]{2,1,0:T(8,128)(2,1)} %fusion.3), calls=%async_computation.2 | async-start | bytes 1048576 | tf_op jit(solution)/shard_map/all_to_all | solution.py:55
  207.4 131.0 %all-gather.5.cloned.1.call-start = ((), (), s32[]{:S(2)}) async-start(), calls=%async_computation.6 | async-start | bytes 3063808 | tf_op jit(solution)/shard_map/all_gather | solution.py:24
  225.9 114.6 %all-to-all-start.3 = ((bf16[16,352,128]{2,1,0:T(8,128)(2,1)}), bf16[16,352,128]{2,1,0:T(8,128)(2,1)S(1)}, u32[]{:S(2)}, u32[]{:S(2)}) async-start(bf16[16,352,128]{2,1,0:T(8,128)(2,1)} %broadcast_in_dim.8), calls=%async_computation.3 | async-start | bytes 2883584 | tf_op jit(solution)/shard_map/all_to_all | solution.py:39
  240.4 4.5 %collective-permute-start.2 = (bf16[8,2048]{1,0:T(8,128)(2,1)S(1)}, bf16[8,2048]{1,0:T(8,128)(2,1)S(1)}, u32[]{:S(2)}, u32[]{:S(2)}) collective-permute-start(bf16[8,2048]{1,0:T(8,128)(2,1)S(1)} %collective-permute-done.1), channel_id=1, source_target_pairs={{0,1},{1,2},{2,3},{3,4},{4,5},{5,6},{6,7},{7,8},{8,9},{9,10},{10,1... | collective-permute-start | bytes 98312 | tf_op jit(solution)/shard_map/ppermute | solution.py:15
  244.9 4.6 %collective-permute-start.3 = (bf16[8,2048]{1,0:T(8,128)(2,1)S(1)}, bf16[8,2048]{1,0:T(8,128)(2,1)S(1)}, u32[]{:S(2)}, u32[]{:S(2)}) collective-permute-start(bf16[8,2048]{1,0:T(8,128)(2,1)S(1)} %collective-permute-done.2), channel_id=1, source_target_pairs={{0,1},{1,2},{2,3},{3,4},{4,5},{5,6},{6,7},{7,8},{8,9},{9,10},{10,1... | collective-permute-start | bytes 98312 | tf_op jit(solution)/shard_map/ppermute | solution.py:15
  249.5 4.7 %collective-permute-start.4 = (bf16[8,2048]{1,0:T(8,128)(2,1)S(1)}, bf16[8,2048]{1,0:T(8,128)(2,1)S(1)}, u32[]{:S(2)}, u32[]{:S(2)}) collective-permute-start(bf16[8,2048]{1,0:T(8,128)(2,1)S(1)} %collective-permute-done.3), channel_id=1, source_target_pairs={{0,1},{1,2},{2,3},{3,4},{4,5},{5,6},{6,7},{7,8},{8,9},{9,10},{10,1... | collective-permute-start | bytes 98312 | tf_op jit(solution)/shard_map/ppermute | solution.py:15
  250.6 4.4 %collective-permute-start.11 = (bf16[8,2048]{1,0:T(8,128)(2,1)S(1)}, bf16[8,2048]{1,0:T(8,128)(2,1)S(1)}, u32[]{:S(2)}, u32[]{:S(2)}) collective-permute-start(bf16[8,2048]{1,0:T(8,128)(2,1)S(1)} %collective-permute-done.10), channel_id=1, source_target_pairs={{0,15},{1,0},{2,1},{3,2},{4,3},{5,4},{6,5},{7,6},{8,7},{9,8},{10,9... | collective-permute-start | bytes 98312 | tf_op jit(solution)/shard_map/ppermute | solution.py:17
  254.2 5.0 %collective-permute-start.5 = (bf16[8,2048]{1,0:T(8,128)(2,1)S(1)}, bf16[8,2048]{1,0:T(8,128)(2,1)S(1)}, u32[]{:S(2)}, u32[]{:S(2)}) collective-permute-start(bf16[8,2048]{1,0:T(8,128)(2,1)S(1)} %collective-permute-done.4), channel_id=1, source_target_pairs={{0,1},{1,2},{2,3},{3,4},{4,5},{5,6},{6,7},{7,8},{8,9},{9,10},{10,1... | collective-permute-start | bytes 98312 | tf_op jit(solution)/shard_map/ppermute | solution.py:15
  255.0 5.0 %collective-permute-start.12 = (bf16[8,2048]{1,0:T(8,128)(2,1)S(1)}, bf16[8,2048]{1,0:T(8,128)(2,1)S(1)}, u32[]{:S(2)}, u32[]{:S(2)}) collective-permute-start(bf16[8,2048]{1,0:T(8,128)(2,1)S(1)} %collective-permute-done.11), channel_id=1, source_target_pairs={{0,15},{1,0},{2,1},{3,2},{4,3},{5,4},{6,5},{7,6},{8,7},{9,8},{10,9... | collective-permute-start | bytes 98312 | tf_op jit(solution)/shard_map/ppermute | solution.py:17
  259.1 5.0 %collective-permute-start.6 = (bf16[8,2048]{1,0:T(8,128)(2,1)S(1)}, bf16[8,2048]{1,0:T(8,128)(2,1)S(1)}, u32[]{:S(2)}, u32[]{:S(2)}) collective-permute-start(bf16[8,2048]{1,0:T(8,128)(2,1)S(1)} %collective-permute-done.5), channel_id=1, source_target_pairs={{0,1},{1,2},{2,3},{3,4},{4,5},{5,6},{6,7},{7,8},{8,9},{9,10},{10,1... | collective-permute-start | bytes 98312 | tf_op jit(solution)/shard_map/ppermute | solution.py:15
  260.0 5.0 %collective-permute-start.13 = (bf16[8,2048]{1,0:T(8,128)(2,1)S(1)}, bf16[8,2048]{1,0:T(8,128)(2,1)S(1)}, u32[]{:S(2)}, u32[]{:S(2)}) collective-permute-start(bf16[8,2048]{1,0:T(8,128)(2,1)S(1)} %collective-permute-done.12), channel_id=1, source_target_pairs={{0,15},{1,0},{2,1},{3,2},{4,3},{5,4},{6,5},{7,6},{8,7},{9,8},{10,9... | collective-permute-start | bytes 98312 | tf_op jit(solution)/shard_map/ppermute | solution.py:17
  264.1 5.0 %collective-permute-start.7 = (bf16[8,2048]{1,0:T(8,128)(2,1)S(1)}, bf16[8,2048]{1,0:T(8,128)(2,1)S(1)}, u32[]{:S(2)}, u32[]{:S(2)}) collective-permute-start(bf16[8,2048]{1,0:T(8,128)(2,1)S(1)} %collective-permute-done.6), channel_id=1, source_target_pairs={{0,1},{1,2},{2,3},{3,4},{4,5},{5,6},{6,7},{7,8},{8,9},{9,10},{10,1... | collective-permute-start | bytes 98312 | tf_op jit(solution)/shard_map/ppermute | solution.py:15
  264.9 5.0 %collective-permute-start.14 = (bf16[8,2048]{1,0:T(8,128)(2,1)S(1)}, bf16[8,2048]{1,0:T(8,128)(2,1)S(1)}, u32[]{:S(2)}, u32[]{:S(2)}) collective-permute-start(bf16[8,2048]{1,0:T(8,128)(2,1)S(1)} %collective-permute-done.13), channel_id=1, source_target_pairs={{0,15},{1,0},{2,1},{3,2},{4,3},{5,4},{6,5},{7,6},{8,7},{9,8},{10,9... | collective-permute-start | bytes 98312 | tf_op jit(solution)/shard_map/ppermute | solution.py:17
  384.0 4.6 %collective-permute-start.18 = (bf16[8,2048]{1,0:T(8,128)(2,1)S(1)}, bf16[8,2048]{1,0:T(8,128)(2,1)S(1)}, u32[]{:S(2)}, u32[]{:S(2)}) collective-permute-start(bf16[8,2048]{1,0:T(8,128)(2,1)S(1)} %collective-permute-done.17), channel_id=1, source_target_pairs={{0,1},{1,2},{2,3},{3,4},{4,5},{5,6},{6,7},{7,8},{8,9},{9,10},{10,1... | collective-permute-start | bytes 98312 | tf_op jit(solution)/shard_map/ppermute | solution.py:15
  388.6 4.6 %collective-permute-start.19 = (bf16[8,2048]{1,0:T(8,128)(2,1)S(1)}, bf16[8,2048]{1,0:T(8,128)(2,1)S(1)}, u32[]{:S(2)}, u32[]{:S(2)}) collective-permute-start(bf16[8,2048]{1,0:T(8,128)(2,1)S(1)} %collective-permute-done.18), channel_id=1, source_target_pairs={{0,1},{1,2},{2,3},{3,4},{4,5},{5,6},{6,7},{7,8},{8,9},{9,10},{10,1... | collective-permute-start | bytes 98312 | tf_op jit(solution)/shard_map/ppermute | solution.py:15
  393.1 4.6 %collective-permute-start.20 = (bf16[8,2048]{1,0:T(8,128)(2,1)S(1)}, bf16[8,2048]{1,0:T(8,128)(2,1)S(1)}, u32[]{:S(2)}, u32[]{:S(2)}) collective-permute-start(bf16[8,2048]{1,0:T(8,128)(2,1)S(1)} %collective-permute-done.19), channel_id=1, source_target_pairs={{0,1},{1,2},{2,3},{3,4},{4,5},{5,6},{6,7},{7,8},{8,9},{9,10},{10,1... | collective-permute-start | bytes 98312 | tf_op jit(solution)/shard_map/ppermute | solution.py:15
  393.3 4.6 %collective-permute-start.27 = (bf16[8,2048]{1,0:T(8,128)(2,1)S(1)}, bf16[8,2048]{1,0:T(8,128)(2,1)S(1)}, u32[]{:S(2)}, u32[]{:S(2)}) collective-permute-start(bf16[8,2048]{1,0:T(8,128)(2,1)S(1)} %collective-permute-done.26), channel_id=1, source_target_pairs={{0,15},{1,0},{2,1},{3,2},{4,3},{5,4},{6,5},{7,6},{8,7},{9,8},{10,9... | collective-permute-start | bytes 98312 | tf_op jit(solution)/shard_map/ppermute | solution.py:17
  397.7 4.6 %collective-permute-start.21 = (bf16[8,2048]{1,0:T(8,128)(2,1)S(1)}, bf16[8,2048]{1,0:T(8,128)(2,1)S(1)}, u32[]{:S(2)}, u32[]{:S(2)}) collective-permute-start(bf16[8,2048]{1,0:T(8,128)(2,1)S(1)} %collective-permute-done.20), channel_id=1, source_target_pairs={{0,1},{1,2},{2,3},{3,4},{4,5},{5,6},{6,7},{7,8},{8,9},{9,10},{10,1... | collective-permute-start | bytes 98312 | tf_op jit(solution)/shard_map/ppermute | solution.py:15
  397.9 4.6 %collective-permute-start.28 = (bf16[8,2048]{1,0:T(8,128)(2,1)S(1)}, bf16[8,2048]{1,0:T(8,128)(2,1)S(1)}, u32[]{:S(2)}, u32[]{:S(2)}) collective-permute-start(bf16[8,2048]{1,0:T(8,128)(2,1)S(1)} %collective-permute-done.27), channel_id=1, source_target_pairs={{0,15},{1,0},{2,1},{3,2},{4,3},{5,4},{6,5},{7,6},{8,7},{9,8},{10,9... | collective-permute-start | bytes 98312 | tf_op jit(solution)/shard_map/ppermute | solution.py:17
  402.2 4.6 %collective-permute-start.22 = (bf16[8,2048]{1,0:T(8,128)(2,1)S(1)}, bf16[8,2048]{1,0:T(8,128)(2,1)S(1)}, u32[]{:S(2)}, u32[]{:S(2)}) collective-permute-start(bf16[8,2048]{1,0:T(8,128)(2,1)S(1)} %collective-permute-done.21), channel_id=1, source_target_pairs={{0,1},{1,2},{2,3},{3,4},{4,5},{5,6},{6,7},{7,8},{8,9},{9,10},{10,1... | collective-permute-start | bytes 98312 | tf_op jit(solution)/shard_map/ppermute | solution.py:15
  402.4 4.6 %collective-permute-start.29 = (bf16[8,2048]{1,0:T(8,128)(2,1)S(1)}, bf16[8,2048]{1,0:T(8,128)(2,1)S(1)}, u32[]{:S(2)}, u32[]{:S(2)}) collective-permute-start(bf16[8,2048]{1,0:T(8,128)(2,1)S(1)} %collective-permute-done.28), channel_id=1, source_target_pairs={{0,15},{1,0},{2,1},{3,2},{4,3},{5,4},{6,5},{7,6},{8,7},{9,8},{10,9... | collective-permute-start | bytes 98312 | tf_op jit(solution)/shard_map/ppermute | solution.py:17
  (22 other events, 649.9 us)
Sparse Core Ops, SparseCore 0:
  56.0 129.4 all-gather.2
  210.3 128.1 all-gather.4
